TPU v7x, 32 devices: a whole 2x2x4 slice. The times are simulated.
32 devices in a mesh: sp: 8 (over z, y), tp: 4 (over x, core).
Axes of the slice: x: 2, y: 2, z: 4, core: 2. Of those that a mesh axis runs over, the one named last changes fastest.
Arguments:
- stream: bfloat16 [2048, 2048], P('sp', 'tp'), may hold values from -6 to 6
- norm_gain: float32 [2, 2048], replicated, may hold values from 0.1 to 1.9
- w_value: bfloat16 [2, 2048, 1024], P(None, 'sp', 'tp'), may hold values from -0.125 to 0.125
- w_gate: bfloat16 [2, 2048, 1024], P(None, 'sp', 'tp'), may hold values from -0.125 to 0.125
- conv_taps: float32 [2, 128, 1024], P(None, None, 'tp'), as said below
- channel_gain: float32 [2, 1024], P(None, 'tp'), may hold values from 0.1 to 1.9
- w_out: bfloat16 [2, 1024, 2048], P(None, 'tp', 'sp'), may hold values from -0.1875 to 0.1875
Outputs:
- result: bfloat16 [2048, 2048], P('sp', 'tp')
Inputs may be any that keep to these rules, and one draw needn't show every extreme that they name: `conv_taps`: taps of each block of 128 consecutive channels share a scale factor of its own.
All inputs are finite; a program needn't handle non-finite values.
Results may differ from a plain program's by a relative error of at most 0.012.
Values may be sent and summed in bfloat16 or wider, within the bound.
A program may use at most 64 MiB of HBM per device.

v0:
```python
import jax
import jax.numpy as jnp
from jax import lax
from jax.sharding import PartitionSpec as P

C = 1024
LAYERS = 2


def from_behind(value, axis, steps):
    count = lax.axis_size(axis)
    initial, last = (max(0, -steps), min(count, count - steps))
    return lax.ppermute(value, axis, [(source, source + steps) for source in range(initial, last)])


def shards(stream, norm_gain, w_value, w_gate, conv_taps, channel_gain, w_out):
    x = stream
    tokens_here = stream.shape[0]
    local_ch = w_value.shape[2]
    taps = conv_taps.shape[1]
    for layer in range(LAYERS):
        whole = lax.all_gather(x, "tp", axis=1, tiled=True).astype(jnp.float32)
        normed = (
            whole
            * lax.rsqrt(jnp.mean(whole * whole, axis=1, keepdims=True) + 1e-06)
            * norm_gain[layer]
        ).astype(jnp.bfloat16)
        value_whole, gate_whole = (
            lax.all_gather(w_value[layer], "sp", axis=0, tiled=True),
            lax.all_gather(w_gate[layer], "sp", axis=0, tiled=True),
        )
        value = jnp.dot(normed, value_whole, preferred_element_type=jnp.float32)
        gate = jnp.dot(normed, gate_whole, preferred_element_type=jnp.float32)
        glu = (value * jax.nn.sigmoid(gate)).astype(jnp.bfloat16)
        before = from_behind(glu[tokens_here - taps :], "sp", 1)
        padded = jnp.concatenate([before[1:], glu], axis=0).astype(jnp.float32)
        conv = lax.conv_general_dilated(
            padded[None],
            conv_taps[layer][:, None, :],
            (1,),
            "VALID",
            dimension_numbers=("NWC", "WIO", "NWC"),
            feature_group_count=local_ch,
            precision=lax.Precision.HIGHEST,
        )[0]
        mean = lax.psum(jnp.sum(conv, axis=1, keepdims=True), "tp") / C
        centred = conv - mean
        spread = lax.psum(jnp.sum(centred * centred, axis=1, keepdims=True), "tp") / C
        act = jax.nn.silu(centred * lax.rsqrt(spread + 1e-05) * channel_gain[layer]).astype(
            jnp.bfloat16
        )
        out_whole = lax.all_gather(w_out[layer], "sp", axis=1, tiled=True)
        terms = jnp.dot(act, out_whole, preferred_element_type=jnp.float32)
        branch = lax.psum_scatter(terms, "tp", scatter_dimension=1, tiled=True)
        x = (x.astype(jnp.float32) + branch).astype(jnp.bfloat16)
    return x


def solution(mesh):
    return jax.shard_map(
        shards,
        mesh=mesh,
        in_specs=(
            P("sp", "tp"),
            P(),
            P(None, "sp", "tp"),
            P(None, "sp", "tp"),
            P(None, None, "tp"),
            P(None, "tp"),
            P(None, "tp", "sp"),
        ),
        out_specs=P("sp", "tp"),
        check_vma=False,
    )
```

profile of v0, /device:TPU:0, one launch (start us, length us, event | category | flops | bytes accessed | tf_op | source)
XLA Modules:
  0.0 370.0 jit_solution(6867189528916284857)
XLA Ops:
  12.7 15.7 %all-gather.15.cloned.1.call-done = bf16[256,2048]{1,0:T(8,128)(2,1)} async-done(((bf16[256,512]{1,0:T(8,128)(2,1)}), bf16[256,2048]{1,0:T(8,128)(2,1)}) %all-gather.15.cloned.1.call-update) | async-done | bytes 1048592 | tf_op jit(solution)/shard_map/all_gather | solution.py:22
  30.0 40.8 %all-gather.19.cloned.1.call-done = bf16[1,2048,256]{2,1,0:T(8,128)(2,1)} async-done(((bf16[1,256,256]{2,1,0:T(8,128)(2,1)}), bf16[1,2048,256]{2,1,0:T(8,128)(2,1)}) %all-gather.19.cloned.1.call-update) | async-done | bytes 1048592 | tf_op jit(solution)/shard_map/all_gather | solution.py:29
  70.8 2.0 fusion.24
  72.8 39.1 %all-gather.21.cloned.1.call-done = bf16[1,2048,256]{2,1,0:T(8,128)(2,1)} async-done(((bf16[1,256,256]{2,1,0:T(8,128)(2,1)}), bf16[1,2048,256]{2,1,0:T(8,128)(2,1)}) %all-gather.21.cloned.1.call-update) | async-done | bytes 1048592 | tf_op jit(solution)/shard_map/all_gather | solution.py:30
  113.7 2.5 collective-permute-start
  116.2 1.9 collective-permute-done
  118.1 4.8 %fusion.50 = (f32[256]{0:T(256)S(1)}, f32[1,256,256]{2,0,1:T(1,128)S(1)}) fusion(f32[1,128,256]{2,1,0:T(8,128)S(1)} %get-tuple-element.6, bf16[1,383,256]{2,1,0:T(8,128)(2,1)S(1)} %maximum_bitcast_fusion), kind=kOutput, calls=%fused_computation.70 | convolution fusion | flops 100728576 | bytes 590336 | tf_op jit(solution)/shard_map/conv_general_dilated | solution.py:37
  123.0 5.7 %psum.28 = f32[256,1]{0,1:T(1,128)S(1)} all-reduce(f32[256,1]{0,1:T(1,128)S(1)} %bitcast.72), channel_id=1, replica_groups=mesh['sp'=8,'tp'=4] {'tp'}, use_global_device_ids=true, to_apply=%region_2.0 | all-reduce | flops 256 | bytes 2048 | tf_op jit(solution)/shard_map/psum | solution.py:46
  128.8 7.0 %psum.29 = f32[256,1]{0,1:T(1,128)S(1)} all-reduce(f32[256,1]{0,1:T(1,128)S(1)} %bitcast.68), channel_id=1, replica_groups=mesh['sp'=8,'tp'=4] {'tp'}, use_global_device_ids=true, to_apply=%region_4.0 | all-reduce | flops 256 | bytes 2048 | tf_op jit(solution)/shard_map/psum | solution.py:48
  135.8 16.2 %all-gather.23.cloned.1.call-done = bf16[1,256,2048]{2,1,0:T(8,128)(2,1)} async-done(((bf16[1,256,256]{2,1,0:T(8,128)(2,1)}), bf16[1,256,2048]{2,1,0:T(8,128)(2,1)}) %all-gather.23.cloned.1.call-update) | async-done | bytes 1048592 | tf_op jit(solution)/shard_map/all_gather | solution.py:52
  152.0 3.1 fusion.21
  155.2 30.3 %reduce-scatter.3.cloned.1.call-done = f32[256,512]{1,0:T(8,128)} async-done(((f32[256,2048]{1,0:T(8,128)}), f32[256,512]{1,0:T(8,128)}) %reduce-scatter.3.cloned.1.call-update) | async-done | bytes 524304 | tf_op jit(solution)/shard_map/reduce_scatter | solution.py:54
  189.6 14.6 %all-gather.17.cloned.1.call-done = bf16[256,2048]{1,0:T(8,128)(2,1)} async-done(((bf16[256,512]{1,0:T(8,128)(2,1)}), bf16[256,2048]{1,0:T(8,128)(2,1)}) %all-gather.17.cloned.1.call-update) | async-done | bytes 1048592 | tf_op jit(solution)/shard_map/all_gather | solution.py:22
  205.8 40.8 %all-gather.25.cloned.1.call-done = bf16[1,2048,256]{2,1,0:T(8,128)(2,1)} async-done(((bf16[1,256,256]{2,1,0:T(8,128)(2,1)}), bf16[1,2048,256]{2,1,0:T(8,128)(2,1)}) %all-gather.25.cloned.1.call-update) | async-done | bytes 1048592 | tf_op jit(solution)/shard_map/all_gather | solution.py:29
  246.6 2.0 fusion.19
  248.6 39.1 %all-gather.27.cloned.1.call-done = bf16[1,2048,256]{2,1,0:T(8,128)(2,1)} async-done(((bf16[1,256,256]{2,1,0:T(8,128)(2,1)}), bf16[1,2048,256]{2,1,0:T(8,128)(2,1)}) %all-gather.27.cloned.1.call-update) | async-done | bytes 1048592 | tf_op jit(solution)/shard_map/all_gather | solution.py:30
  289.5 2.5 collective-permute-start.1
  292.0 1.9 collective-permute-done.1
  293.9 4.8 %fusion.51 = (f32[256]{0:T(256)S(1)}, f32[1,256,256]{2,0,1:T(1,128)S(1)}) fusion(f32[1,128,256]{2,1,0:T(8,128)S(1)} %get-tuple-element.5, bf16[1,383,256]{2,1,0:T(8,128)(2,1)S(1)} %maximum_bitcast_fusion.1), kind=kOutput, calls=%fused_computation.71 | convolution fusion | flops 100728576 | bytes 590336 | tf_op jit(solution)/shard_map/conv_general_dilated | solution.py:37
  298.8 5.7 %psum.30 = f32[256,1]{0,1:T(1,128)S(1)} all-reduce(f32[256,1]{0,1:T(1,128)S(1)} %bitcast.73), channel_id=1, replica_groups=mesh['sp'=8,'tp'=4] {'tp'}, use_global_device_ids=true, to_apply=%region_8.9 | all-reduce | flops 256 | bytes 2048 | tf_op jit(solution)/shard_map/psum | solution.py:46
  304.6 7.0 %psum.31 = f32[256,1]{0,1:T(1,128)S(1)} all-reduce(f32[256,1]{0,1:T(1,128)S(1)} %bitcast.69), channel_id=1, replica_groups=mesh['sp'=8,'tp'=4] {'tp'}, use_global_device_ids=true, to_apply=%region_10.11 | all-reduce | flops 256 | bytes 2048 | tf_op jit(solution)/shard_map/psum | solution.py:48
  311.6 16.3 %all-gather.29.cloned.1.call-done = bf16[1,256,2048]{2,1,0:T(8,128)(2,1)} async-done(((bf16[1,256,256]{2,1,0:T(8,128)(2,1)}), bf16[1,256,2048]{2,1,0:T(8,128)(2,1)}) %all-gather.29.cloned.1.call-update) | async-done | bytes 1048592 | tf_op jit(solution)/shard_map/all_gather | solution.py:52
  327.9 3.1 fusion.16
  331.1 30.3 %reduce-scatter.5.cloned.1.call-done = f32[256,512]{1,0:T(8,128)} async-done(((f32[256,2048]{1,0:T(8,128)}), f32[256,512]{1,0:T(8,128)}) %reduce-scatter.5.cloned.1.call-update) | async-done | bytes 524304 | tf_op jit(solution)/shard_map/reduce_scatter | solution.py:54
  (60 shorter events, 19.2 us)
Async XLA Ops:
  6.5 6.1 %copy-start.5 = (f32[2,2048]{1,0:T(2,128)S(1)}, f32[2,2048]{1,0:T(2,128)}, u32[]{:S(2)}) copy-start(f32[2,2048]{1,0:T(2,128)} %param.8) | copy-start | bytes 49156
  6.5 6.1 %copy-start.4 = (f32[2,128,256]{2,1,0:T(8,128)S(1)}, f32[2,128,256]{2,1,0:T(8,128)}, u32[]{:S(2)}) copy-start(f32[2,128,256]{2,1,0:T(8,128)} %param.11) | copy-start | bytes 786436
  6.5 21.8 %all-gather.15.cloned.1.call-start = ((), (), s32[]{:S(2)}) async-start(), calls=%async_computation.2 | async-start | bytes 1310720 | tf_op jit(solution)/shard_map/all_gather | solution.py:22
  7.3 63.5 %all-gather.19.cloned.1.call-start = ((), (), s32[]{:S(2)}) async-start(), calls=%async_computation.6 | async-start | bytes 1179648 | tf_op jit(solution)/shard_map/all_gather | solution.py:29
  9.0 102.9 %all-gather.21.cloned.1.call-start = ((), (), s32[]{:S(2)}) async-start(), calls=%async_computation.7 | async-start | bytes 1179648 | tf_op jit(solution)/shard_map/all_gather | solution.py:30
  10.8 141.2 %all-gather.23.cloned.1.call-start = ((), (), s32[]{:S(2)}) async-start(), calls=%async_computation.8 | async-start | bytes 1179648 | tf_op jit(solution)/shard_map/all_gather | solution.py:52
  12.6 172.9 %reduce-scatter.3.cloned.1.call-start = ((), (), s32[]{:S(2)}) async-start(), calls=%async_computation.3 | async-start | bytes 2621440 | tf_op jit(solution)/shard_map/reduce_scatter | solution.py:54
  28.4 83.6 %copy-start.1 = (bf16[256,2048]{1,0:T(8,128)(2,1)S(1)}, bf16[256,2048]{1,0:T(8,128)(2,1)}, u32[]{:S(2)}) copy-start(bf16[256,2048]{1,0:T(8,128)(2,1)} %all-gather.15.cloned.1.call-done) | copy-start | bytes 3145732
  72.8 43.4 %copy-start.6 = (f32[2,256]{1,0:T(2,128)S(1)}, f32[2,256]{1,0:T(2,128)}, u32[]{:S(2)}) copy-start(f32[2,256]{1,0:T(2,128)} %param.12) | copy-start | bytes 6148
  113.7 4.4 %collective-permute-start = (bf16[128,256]{1,0:T(8,128)(2,1)S(1)}, bf16[128,256]{1,0:T(8,128)(2,1)S(1)}, u32[]{:S(2)}, u32[]{:S(2)}) collective-permute-start(bf16[128,256]{1,0:T(8,128)(2,1)S(1)} %slice.64), channel_id=1, source_target_pairs={{0,4},{4,8},{8,12},{12,16},{16,20},{20,24},{24,28},{1,5},{5,9},{9,... | collective-permute-start | bytes 196616 | tf_op jit(solution)/shard_map/ppermute | solution.py:13
  152.0 33.5 %copy-start.3 = (bf16[256,512]{1,0:T(8,128)(2,1)S(1)}, bf16[256,512]{1,0:T(8,128)(2,1)}, u32[]{:S(2)}) copy-start(bf16[256,512]{1,0:T(8,128)(2,1)} %param.7) | copy-start | bytes 786436
  155.1 49.0 %all-gather.17.cloned.1.call-start = ((), (), s32[]{:S(2)}) async-start(), calls=%async_computation.4 | async-start | bytes 1310720 | tf_op jit(solution)/shard_map/all_gather | solution.py:22
  187.3 59.3 %all-gather.25.cloned.1.call-start = ((), (), s32[]{:S(2)}) async-start(), calls=%async_computation.9 | async-start | bytes 1179648 | tf_op jit(solution)/shard_map/all_gather | solution.py:29
  188.0 99.7 %all-gather.27.cloned.1.call-start = ((), (), s32[]{:S(2)}) async-start(), calls=%async_computation.10 | async-start | bytes 1179648 | tf_op jit(solution)/shard_map/all_gather | solution.py:30
  188.8 139.1 %all-gather.29.cloned.1.call-start = ((), (), s32[]{:S(2)}) async-start(), calls=%async_computation.11 | async-start | bytes 1179648 | tf_op jit(solution)/shard_map/all_gather | solution.py:52
  189.5 171.9 %reduce-scatter.5.cloned.1.call-start = ((), (), s32[]{:S(2)}) async-start(), calls=%async_computation.5 | async-start | bytes 2621440 | tf_op jit(solution)/shard_map/reduce_scatter | solution.py:54
  204.1 83.6 %copy-start.2 = (bf16[256,2048]{1,0:T(8,128)(2,1)S(1)}, bf16[256,2048]{1,0:T(8,128)(2,1)}, u32[]{:S(2)}) copy-start(bf16[256,2048]{1,0:T(8,128)(2,1)} %all-gather.17.cloned.1.call-done) | copy-start | bytes 3145732
  289.5 4.4 %collective-permute-start.1 = (bf16[128,256]{1,0:T(8,128)(2,1)S(1)}, bf16[128,256]{1,0:T(8,128)(2,1)S(1)}, u32[]{:S(2)}, u32[]{:S(2)}) collective-permute-start(bf16[128,256]{1,0:T(8,128)(2,1)S(1)} %slice.66), channel_id=1, source_target_pairs={{0,4},{4,8},{8,12},{12,16},{16,20},{20,24},{24,28},{1,5},{5,9},{9,... | collective-permute-start | bytes 196616 | tf_op jit(solution)/shard_map/ppermute | solution.py:13
  327.9 33.5 %copy-start = (bf16[256,512]{1,0:T(8,128)(2,1)S(1)}, bf16[256,512]{1,0:T(8,128)(2,1)}, u32[]{:S(2)}) copy-start(bf16[256,512]{1,0:T(8,128)(2,1)} %add_convert_fusion.1) | copy-start | bytes 786436
Sparse Core Ops, SparseCore 0:
  8.9 19.4 all-gather.14
  30.5 40.2 all-gather.18
  72.9 38.9 all-gather.20
  113.8 38.0 all-gather.22
  155.2 30.1 reduce-scatter.2
  187.4 16.6 all-gather.16
  206.3 40.2 all-gather.24
  248.7 38.9 all-gather.26
  289.8 38.0 all-gather.28
  331.2 30.1 reduce-scatter.4
where the time goes:
time: 371 us; the launch traced here: 370 us
  waiting for transfers between devices  290 us (78%)
  blocking collectives  25.3 us (7%)
  matrix products  23.4 us (6%)
  between operations  13.7 us (4%)
  other arithmetic  7.31 us (2%)
  starting transfers between devices  5.32 us (1%)
  local copies, waits for them, and re-layouts  5.19 us (1%)
    all_gather x2, waiting for transfers between devices, shards(): lax.all_gather(w_value[layer], 'sp', axis=0, tiled=True)  81.7 us
    all_gather x2, waiting for transfers between devices, shards(): lax.all_gather(w_gate[layer], 'sp', axis=0, tiled=True)  78.2 us
    reduce_scatter x2, waiting for transfers between devices, shards(): branch = lax.psum_scatter(terms, 'tp', scatter_dimension=1, tiled=True)  60.6 us
    all_gather x2, waiting for transfers between devices, shards(): out_whole = lax.all_gather(w_out[layer], 'sp', axis=1, tiled=True)  32.5 us
    all_gather x2, waiting for transfers between devices, shards(): whole = lax.all_gather(x, 'tp', axis=1, tiled=True).astype(jnp.float32)  30.3 us
    psum x2, blocking collectives, shards(): lax.psum(jnp.sum(centred * centred, axis=1, keepdims=True), 'tp') / C  14 us
    psum x2, blocking collectives, shards(): mean = lax.psum(jnp.sum(conv, axis=1, keepdims=True), 'tp') / C  11.3 us
    conv_general_dilated x2, matrix products, shards(): lax.conv_general_dilated(padded[None], conv_taps[layer][:, None, :], (1,)...  9.67 us
  transfers between devices with their start and end apart: 12, of which 12 were waited for; matrix products, arithmetic and copies ran while one was open for 7% of the time, Pallas kernels for 0%

commit v1 on v0

v1 whole, which is shorter than its diff:
```python
import functools

import jax
import jax.numpy as jnp
from jax import lax
from jax.experimental import pallas as pl
from jax.experimental.pallas import tpu as pltpu
from jax.sharding import PartitionSpec as P

F32, BF16 = jnp.float32, jnp.bfloat16
LANES = 128
ROW_TILE = 16
MESH = pl.DeviceIdType.MESH


def span(masks):
    found = [0]
    for mask in masks:
        found = found + [entry ^ mask for entry in found]
    return found


def parts_of(rows, most):
    parts = most
    while rows % (parts * ROW_TILE):
        parts //= 2
    return parts


def ring_chunks(layers, rows, width):
    stages = []
    for layer in range(layers):
        parts = parts_of(rows, 4)
        step = rows // parts
        stages.append(
            [(which, layer, which, part * step, step, 0, width) for part in range(parts) for which in (0, 1)]
        )
        parts = parts_of(rows, 2)
        step, half = rows // parts, width // 2
        stages.append(
            [(2, layer, way, part * step, step, way * half, half) for part in range(parts) for way in (0, 1)]
        )
    return stages


def kernel(
    count, peers, stages,
    x_ref, gain_ref, wv_ref, wg_ref, taps_ref, channel_ref, wo_ref, out_ref,
    full, gathered, normed, glu, halo, padded, conv, stat, act, mine, leaving, landing, middle,
    ring_send, ring_recv, x_send, x_recv, halo_send, halo_recv, stat_send, stat_recv, sum_send, sum_recv, own_sem,
):
    s, t = lax.axis_index("sp"), lax.axis_index("tp")
    tokens, part = x_ref.shape
    layers, rows, width = wv_ref.shape
    features = rows * count
    taps = taps_ref.shape[1]
    channels = width * peers
    groups = width // LANES
    last = count - 1
    lag = last // 2

    odd = s % 2
    place = (1 - odd) * (s // 2) + odd * (last - s // 2)

    def at_place(where):
        where = (where + count) % count
        upper = where // (count // 2)
        return (1 - upper) * (2 * where) + upper * (2 * (last - where) + 1)

    ahead, behind = at_place(place + 1), at_place(place - 1)
    masks = []
    mask = peers // 2
    while mask:
        masks.append(mask)
        mask //= 2

    def partner(bits):
        other = t
        for mask in masks:
            if bits & mask:
                other = other + mask - 2 * mask * ((t // mask) % 2)
        return other

    after, before = (s + 1) % count, (s + last) % count
    barrier = pltpu.get_barrier_semaphore()
    greeted = [(ahead, t), (behind, t), (after, t), (before, t)]
    greeted += [(s, partner(bits)) for bits in range(1, peers)]
    for who in greeted:
        pl.semaphore_signal(barrier, inc=1, device_id=who, device_id_type=MESH)
    pl.semaphore_wait(barrier, len(greeted))

    sources = (wv_ref, wg_ref, wo_ref)
    own_copies = []
    for which in range(3):
        own = pltpu.make_async_copy(
            sources[which],
            full.at[which, :, pl.ds(pl.multiple_of(s * rows, rows), rows), :],
            own_sem.at[which],
        )
        own.start()
        own_copies.append(own)

    numbered, total = [], 0
    for stage in stages:
        numbered.append([(total + offset, piece) for offset, piece in enumerate(stage)])
        total += len(stage)

    def ring_copy(number, piece, step, first, recv_step):
        which, layer, way, row, height, lane, lanes = piece
        block = at_place(place - step) if way == 0 else at_place(place + step)
        lane_slice = pl.ds(lane, lanes)
        start = pl.multiple_of(block * rows + row, ROW_TILE)
        there = full.at[which, layer, pl.ds(start, height), lane_slice]
        here = sources[which].at[layer, pl.ds(row, height), lane_slice] if first else there
        return pltpu.make_async_remote_copy(
            src_ref=here,
            dst_ref=there,
            send_sem=ring_send.at[number, step],
            recv_sem=ring_recv.at[number, recv_step],
            device_id=((ahead, behind)[way], t),
            device_id_type=MESH,
        )

    offsets = [layer * last + extra for layer in range(layers) for extra in (0, lag)]
    edges = sorted({offset + extra for offset in offsets for extra in (0, 1, last, last + 1)})
    clock = [0]

    def advance(to):
        while clock[0] < to:
            now = clock[0]
            end = min([edge for edge in edges if edge > now] + [to])
            end = min(end, to)
            active = [
                (stage, offset, now - offset)
                for stage, offset in zip(numbered, offsets)
                if 0 <= now - offset <= last
            ]

            def slot(at):
                for stage, offset, shown in active:
                    step = at - offset
                    for number, piece in stage:
                        if shown == 0:
                            ring_copy(number, piece, 0, True, 0).start()
                            continue
                        if shown == last:
                            which, layer, way, row, height, lane, lanes = piece
                            ring_copy(number, piece, last - 1, False, last - 1).wait_recv()
                            continue
                        ring_copy(number, piece, step, False, step - 1).wait_recv()
                        ring_copy(number, piece, step, False, step).start()

            if end - now == 1:
                slot(now)
            else:
                def body(at, carry):
                    slot(at)
                    return carry

                lax.fori_loop(now, end, body, 0)
            clock[0] = end

    def share_copy(layer, source, mask, sub):
        return pltpu.make_async_remote_copy(
            src_ref=source,
            dst_ref=gathered.at[layer, partner(sub)],
            send_sem=x_send.at[layer, mask ^ sub],
            recv_sem=x_recv.at[layer, mask ^ sub],
            device_id=(s, partner(mask)),
            device_id_type=MESH,
        )

    order = [(mask, sub) for place_, mask in enumerate(masks) for sub in span(masks[:place_])]

    def share_start(layer, source):
        for mask in masks:
            share_copy(layer, source, mask, 0).start()
        gathered[layer, t] = source[...]

    def share_relay(layer, source):
        for mask, sub in order:
            if sub:
                got = gathered.at[layer, partner(sub)]
                share_copy(layer, got, mask, sub).start()
            share_copy(layer, source, mask, sub).wait_recv()

    def share_end(layer, source):
        for mask, sub in order:
            share_copy(layer, source, mask, sub).wait_send()

    def normalise(layer):
        squares = jnp.zeros((tokens, 1), F32)
        for block in range(peers):
            value = gathered[layer, block].astype(F32)
            squares += jnp.sum(value * value, axis=1, keepdims=True)
        scale = lax.rsqrt(squares / features + 1e-06)
        for block in range(peers):
            gain = gain_ref[layer : layer + 1, block * part : (block + 1) * part]
            normed[:, block * part : (block + 1) * part] = (
                gathered[layer, block].astype(F32) * scale * gain
            ).astype(BF16)

    def halo_copy(layer):
        return pltpu.make_async_remote_copy(
            src_ref=glu.at[layer, pl.ds(tokens - taps, taps), :],
            dst_ref=halo.at[layer],
            send_sem=halo_send.at[layer],
            recv_sem=halo_recv.at[layer],
            device_id=(after, t),
            device_id_type=MESH,
        )

    def gated(layer):
        value = jnp.dot(normed[...], full[0, layer], preferred_element_type=F32)
        gate = jnp.dot(normed[...], full[1, layer], preferred_element_type=F32)
        rounded = (value * jax.nn.sigmoid(gate)).astype(BF16)
        glu[layer] = rounded

        @pl.when(s < last)
        def _():
            halo_copy(layer).start()

        wide = rounded.astype(F32)
        for group in range(groups):
            padded[group, taps:, :] = wide[:, group * LANES : (group + 1) * LANES]

    def halo_arrive(layer):
        @pl.when(s > 0)
        def _():
            halo_copy(layer).wait_recv()
            wide = halo[layer].astype(F32)
            for group in range(groups):
                padded[group, :taps, :] = wide[:, group * LANES : (group + 1) * LANES]

        @pl.when(s == 0)
        def _():
            padded[:, :taps, :] = jnp.zeros((groups, taps, LANES), F32)

    half = tokens // 2

    def convolve(layer, which):
        for group in range(groups):
            lanes = slice(group * LANES, (group + 1) * LANES)

            def body(block, total, group=group, lanes=lanes):
                eight = taps_ref[layer, pl.ds(pl.multiple_of(block * 8, 8), 8), lanes]
                for unit in range(8):
                    total += eight[unit : unit + 1] * padded[group, pl.ds(which * half + block * 8 + unit + 1, half), :]
                return total

            conv[which * half : (which + 1) * half, lanes] = lax.fori_loop(
                0, taps // 8, body, jnp.zeros((half, LANES), F32)
            )

    def stat_copy(layer, bits):
        return pltpu.make_async_remote_copy(
            src_ref=stat.at[layer, t],
            dst_ref=stat.at[layer, t],
            send_sem=stat_send.at[layer, bits],
            recv_sem=stat_recv.at[layer, bits],
            device_id=(s, partner(bits)),
            device_id_type=MESH,
        )

    def stat_start(layer):
        value = conv[...]
        sums = jnp.sum(value, axis=1, keepdims=True)
        centred = value - sums / width
        squares = jnp.sum(centred * centred, axis=1, keepdims=True)
        lane = lax.broadcasted_iota(jnp.int32, (tokens, LANES), 1)
        packed = jnp.where(lane == 0, sums, jnp.where(lane == 1, squares, 0.0))
        stat[layer, t] = packed.T[:8, :]
        for bits in range(1, peers):
            stat_copy(layer, bits).start()

    def activate(layer):
        for bits in range(1, peers):
            stat_copy(layer, bits).wait_recv()
        every = [stat[layer, block] for block in range(peers)]
        mean = sum(entry[0:1] for entry in every) / channels
        squares = sum(
            entry[1:2] + width * (entry[0:1] / width - mean) * (entry[0:1] / width - mean) for entry in every
        )
        scale = lax.rsqrt(squares / channels + 1e-05)
        row = lax.broadcasted_iota(jnp.int32, (LANES, tokens), 0)
        columns = jnp.where(row == 0, mean, jnp.where(row == 1, scale, 0.0)).T
        v = (conv[...] - columns[:, 0:1]) * columns[:, 1:2] * channel_ref[layer : layer + 1, :]
        act[...] = (v * jax.nn.sigmoid(v)).astype(BF16)

    def sum_copy(layer, mask, sub):
        return pltpu.make_async_remote_copy(
            src_ref=leaving.at[layer, mask ^ sub],
            dst_ref=landing.at[layer, mask ^ sub],
            send_sem=sum_send.at[layer, mask ^ sub],
            recv_sem=sum_recv.at[layer, mask ^ sub],
            device_id=(s, partner(mask)),
            device_id_type=MESH,
        )

    rising = masks[::-1]

    def product(layer, bits):
        start = pl.multiple_of(partner(bits) * part, part)
        return lax.dot_general(
            act[...],
            full[2, layer, pl.ds(start, part), :],
            (((1,), (1,)), ((), ())),
            preferred_element_type=F32,
        )

    def reduce_start(layer):
        mask = rising[0]
        subs = span(rising[1:])[::-1]
        for sub in subs:
            leaving[layer, mask ^ sub] = product(layer, mask ^ sub).astype(BF16)
            sum_copy(layer, mask, sub).start()
        for sub in subs:
            mine[sub] = product(layer, sub)
            sum_copy(layer, mask, sub).wait_recv()
            mine[sub] = mine[sub] + landing[layer, mask ^ sub].astype(F32)
            if len(rising) > 1 and sub & rising[1]:
                leaving[layer, sub] = mine[sub].astype(BF16)
                sum_copy(layer, rising[1], sub ^ rising[1]).start()

    def reduce_end(layer, source, target):
        for level in range(1, len(rising)):
            mask = rising[level]
            for sub in span(rising[level + 1 :])[::-1]:
                sum_copy(layer, mask, sub).wait_recv()
                mine[sub] = mine[sub] + landing[layer, mask ^ sub].astype(F32)
                if level + 1 < len(rising) and sub & rising[level + 1]:
                    leaving[layer, sub] = mine[sub].astype(BF16)
                    sum_copy(layer, rising[level + 1], sub ^ rising[level + 1]).start()
        target[...] = (source[...].astype(F32) + mine[0]).astype(BF16)

    current = x_ref
    share_start(0, current)
    advance(min(3, last))
    share_relay(0, current)
    advance(min(4, last))
    normalise(0)
    for layer in range(layers):
        base = (layer + 1) * last
        if layer == 0:
            for own in own_copies:
                own.wait()
        advance(base + 1)
        gated(layer)
        advance(base + 2)
        halo_arrive(layer)
        convolve(layer, 0)
        advance(base + min(3, lag))
        convolve(layer, 1)
        stat_start(layer)
        advance(base + lag + 1)
        activate(layer)
        reduce_start(layer)
        if layer + 1 < layers:
            advance(base + lag + 2)
            reduce_end(layer, current, middle.at[layer])
            current = middle.at[layer]
            share_start(layer + 1, current)
            advance(base + lag + 3)
            share_relay(layer + 1, current)
            normalise(layer + 1)
        else:
            reduce_end(layer, current, out_ref)

    for layer in range(layers):
        source = x_ref if layer == 0 else middle.at[layer - 1]
        share_end(layer, source)
        for bits in range(1, peers):
            stat_copy(layer, bits).wait_send()
        for level, mask in enumerate(rising):
            for sub in span(rising[level + 1 :]):
                sum_copy(layer, mask, sub).wait_send()

        @pl.when(s < last)
        def _(layer=layer):
            halo_copy(layer).wait_send()

    def drain(step, carry):
        for stage in numbered:
            for number, piece in stage:
                ring_copy(number, piece, step, False, step).wait_send()
        return carry

    lax.fori_loop(0, last, drain, 0)


def shards(count, peers, stream, norm_gain, w_value, w_gate, conv_taps, channel_gain, w_out):
    tokens, part = stream.shape
    layers, rows, width = w_value.shape
    taps = conv_taps.shape[1]
    features = rows * count
    stages = ring_chunks(layers, rows, width)
    pieces = sum(len(stage) for stage in stages)
    dma = pltpu.SemaphoreType.DMA
    return pl.pallas_call(
        functools.partial(kernel, count, peers, stages),
        out_shape=jax.ShapeDtypeStruct((tokens, part), BF16),
        in_specs=[pl.BlockSpec(memory_space=pltpu.VMEM)] * 7,
        out_specs=pl.BlockSpec(memory_space=pltpu.VMEM),
        scratch_shapes=[
            pltpu.VMEM((3, layers, features, width), BF16),
            pltpu.VMEM((layers, peers, tokens, part), BF16),
            pltpu.VMEM((tokens, features), BF16),
            pltpu.VMEM((layers, tokens, width), BF16),
            pltpu.VMEM((layers, taps, width), BF16),
            pltpu.VMEM((width // LANES, taps + tokens, LANES), F32),
            pltpu.VMEM((tokens, width), F32),
            pltpu.VMEM((layers, peers, 8, tokens), F32),
            pltpu.VMEM((tokens, width), BF16),
            pltpu.VMEM((peers, tokens, part), F32),
            pltpu.VMEM((layers, peers, tokens, part), BF16),
            pltpu.VMEM((layers, peers, tokens, part), BF16),
            pltpu.VMEM((layers, tokens, part), BF16),
            dma((pieces, count - 1)),
            dma((pieces, count - 1)),
            dma((layers, peers)),
            dma((layers, peers)),
            dma((layers,)),
            dma((layers,)),
            dma((layers, peers)),
            dma((layers, peers)),
            dma((layers, peers)),
            dma((layers, peers)),
            dma((3,)),
        ],
        compiler_params=pltpu.CompilerParams(
            collective_id=0, has_side_effects=True, vmem_limit_bytes=60 * 1024 * 1024
        ),
    )(stream, norm_gain, w_value, w_gate, conv_taps, channel_gain, jnp.swapaxes(w_out, 1, 2))


def solution(mesh):
    return jax.shard_map(
        functools.partial(shards, mesh.shape["sp"], mesh.shape["tp"]),
        mesh=mesh,
        in_specs=(
            P("sp", "tp"),
            P(),
            P(None, "sp", "tp"),
            P(None, "sp", "tp"),
            P(None, None, "tp"),
            P(None, "tp"),
            P(None, "tp", "sp"),
        ),
        out_specs=P("sp", "tp"),
        check_vma=False,
    )
```

time: 371 us -> 105 us (0.28)
  waiting for transfers between devices: 290 us -> 0 us
  Pallas kernels: 0 us -> 101 us
  blocking collectives: 25.3 us -> 0 us
  matrix products: 23.4 us -> 0 us
  between operations: 13.7 us -> 0.01 us
  other arithmetic: 7.31 us -> 0 us
  starting transfers between devices: 5.32 us -> 0 us
    all_gather x8 -> x0, waiting for transfers between devices: 223 us -> none  [the longest x2 81.7 us: shards(): lax.all_gather(w_value[layer], 'sp', axis=0, tiled=True)]
    pallas_call x0 -> x1, Pallas kernels: none -> 101 us  [shards(): pl.pallas_call(functools.partial(kernel, count, peers, stages), out_shape...]
    reduce_scatter x2 -> x0, waiting for transfers between devices: 60.6 us -> none  [shards(): branch = lax.psum_scatter(terms, 'tp', scatter_dimension=1, tiled=True)]
    psum x4 -> x0, blocking collectives: 25.3 us -> none  [the longest x2 14 us: shards(): lax.psum(jnp.sum(centred * centred, axis=1, keepdims=True), 'tp') / C]
    dot_general x6 -> x0, matrix products: 13.7 us -> none  [the longest x2 6.22 us: shards(): terms = jnp.dot(act, out_whole, preferred_element_type=jnp.float32)]
    conv_general_dilated x2 -> x0, matrix products: 9.67 us -> none  [shards(): lax.conv_general_dilated(padded[None], conv_taps[layer][:, None, :], (1,)...]
    slice x10 -> x0, local copies, waits for them, and re-layouts: 5.16 us -> none  [the longest x1 1.7 us: shards(): w_value[layer]]
    ppermute x2 -> x0, starting transfers between devices: 4.96 us -> none  [from_behind(): lax.ppermute(value, axis, [(source, source + steps) for source in range(i...]
  transfers between devices with their start and end apart: 12 -> 0, of which waited for: 12 -> 0; matrix products, arithmetic and copies ran while one was open for 7% -> 0% of each run, Pallas kernels for 0% -> 0%
where the time goes in v1:
time: 105 us; the launch traced here: 104 us
  Pallas kernels  101 us (96%)
  local copies, waits for them, and re-layouts  3.46 us (3%)
    pallas_call x1, Pallas kernels, shards(): pl.pallas_call(functools.partial(kernel, count, peers, stages), out_shape...  101 us
    unnamed x2, local copies, waits for them, and re-layouts  3.46 us

profile of v1, /device:TPU:0, one launch (start us, length us, event | category | flops | bytes accessed | tf_op | source)
XLA Modules:
  0.0 104.5 jit_solution(16070708462368194886)
XLA Ops:
  0.0 1.8 %copy.8 = bf16[2,256,256]{1,2,0:T(8,128)(2,1)} copy(bf16[2,256,256]{2,1,0:T(8,128)(2,1)} %param.13) | data formatting | bytes 524288 | tf_op args[6]
  1.8 101.0 %shard_map.73 = bf16[256,512]{1,0:T(8,128)(2,1)} custom-call(bf16[256,512]{1,0:T(8,128)(2,1)} %x_ref.1, f32[2,2048]{1,0:T(2,128)} %gain_ref.1, bf16[2,256,256]{2,1,0:T(8,128)(2,1)} %wv_ref.1, bf16[2,256,256]{2,1,0:T(8,128)(2,1)} %wg_ref.1, f32[2,128,256]{2,1,0:T(8,128)} %taps_ref.1, f32[2,256]{1,0:T(2,128)} %channel_ref.1, bf16[2,256,256]{2,1,0:T(8,128)(2,1)} %bitcast.1), custom_call_target="tpu_custom_call" | custom-call | tf_op jit(solution)/shard_map/pallas_call | solution.py:399
  102.8 1.7 %copy.10 = bf16[256,512]{1,0:T(8,128)(2,1)} copy(bf16[256,512]{1,0:T(8,128)(2,1)} %shard_map.73) | data formatting | bytes 524288

commit v2 on v1

--- a/solution.py
+++ b/solution.py
@@ -11,6 +11,7 @@
 LANES = 128
 ROW_TILE = 16
 MESH = pl.DeviceIdType.MESH
+PLAN = (3, 0, 3, 1, 2, 2, 2)
 
 
 def span(masks):
@@ -27,7 +28,7 @@
     return parts
 
 
-def ring_chunks(layers, rows, width):
+def ring_chunks(layers, rows, width, columns):
     stages = []
     for layer in range(layers):
         parts = parts_of(rows, 4)
@@ -35,10 +36,15 @@
         stages.append(
             [(which, layer, which, part * step, step, 0, width) for part in range(parts) for which in (0, 1)]
         )
-        parts = parts_of(rows, 2)
-        step, half = rows // parts, width // 2
+        parts = parts_of(width, 4) if columns % LANES == 0 else 2
+        high, step = (width // parts, columns) if columns % LANES == 0 else (rows, width // parts)
         stages.append(
-            [(2, layer, way, part * step, step, way * half, half) for part in range(parts) for way in (0, 1)]
+            [
+                (2, layer, part % 2, part * high, high, 0, step)
+                if columns % LANES == 0
+                else (2, layer, part % 2, 0, high, part * step, step)
+                for part in range(parts)
+            ]
         )
     return stages
 
@@ -46,7 +52,7 @@
 def kernel(
     count, peers, stages,
     x_ref, gain_ref, wv_ref, wg_ref, taps_ref, channel_ref, wo_ref, out_ref,
-    full, gathered, normed, glu, halo, padded, conv, stat, act, mine, leaving, landing, middle,
+    full, full_out, gathered, normed, glu, halo, padded, conv, stat, act, mine, leaving, landing, middle,
     ring_send, ring_recv, x_send, x_recv, halo_send, halo_recv, stat_send, stat_recv, sum_send, sum_recv, own_sem,
 ):
     s, t = lax.axis_index("sp"), lax.axis_index("tp")
@@ -57,7 +63,6 @@
     channels = width * peers
     groups = width // LANES
     last = count - 1
-    lag = last // 2
 
     odd = s % 2
     place = (1 - odd) * (s // 2) + odd * (last - s // 2)
@@ -92,11 +97,8 @@
     sources = (wv_ref, wg_ref, wo_ref)
     own_copies = []
     for which in range(3):
-        own = pltpu.make_async_copy(
-            sources[which],
-            full.at[which, :, pl.ds(pl.multiple_of(s * rows, rows), rows), :],
-            own_sem.at[which],
-        )
+        own_place = full.at[which, :, pl.ds(pl.multiple_of(s * rows, rows), rows), :] if which < 2 else full_out.at[:, s]
+        own = pltpu.make_async_copy(sources[which], own_place, own_sem.at[which])
         own.start()
         own_copies.append(own)
 
@@ -109,8 +111,11 @@
         which, layer, way, row, height, lane, lanes = piece
         block = at_place(place - step) if way == 0 else at_place(place + step)
         lane_slice = pl.ds(lane, lanes)
-        start = pl.multiple_of(block * rows + row, ROW_TILE)
-        there = full.at[which, layer, pl.ds(start, height), lane_slice]
+        if which < 2:
+            start = pl.multiple_of(block * rows + row, ROW_TILE)
+            there = full.at[which, layer, pl.ds(start, height), lane_slice]
+        else:
+            there = full_out.at[layer, block, pl.ds(row, height), lane_slice]
         here = sources[which].at[layer, pl.ds(row, height), lane_slice] if first else there
         return pltpu.make_async_remote_copy(
             src_ref=here,
@@ -121,7 +126,12 @@
             device_id_type=MESH,
         )
 
-    offsets = [layer * last + extra for layer in range(layers) for extra in (0, lag)]
+    lag, gap, late, conv_a, conv_b, wait_sum, wait_share = PLAN
+    offsets = [
+        layer * (last + gap) + extra
+        for layer in range(layers)
+        for extra in (0, min(late if layer == layers - 1 else lag, last))
+    ]
     edges = sorted({offset + extra for offset in offsets for extra in (0, 1, last, last + 1)})
     clock = [0]
 
@@ -299,14 +309,19 @@
 
     rising = masks[::-1]
 
+    upright = wo_ref.shape[1] == width and wo_ref.shape[2] % LANES == 0
+    owned = count // peers
+
     def product(layer, bits):
-        start = pl.multiple_of(partner(bits) * part, part)
-        return lax.dot_general(
-            act[...],
-            full[2, layer, pl.ds(start, part), :],
-            (((1,), (1,)), ((), ())),
-            preferred_element_type=F32,
-        )
+        whose = partner(bits)
+        if upright:
+            found = [
+                jnp.dot(act[...], full_out[layer, whose * owned + block], preferred_element_type=F32)
+                for block in range(owned)
+            ]
+            return jnp.concatenate(found, axis=1)
+        found = full_out[layer, pl.ds(whose * owned, owned)].reshape(part, width)
+        return lax.dot_general(act[...], found, (((1,), (1,)), ((), ())), preferred_element_type=F32)
 
     def reduce_start(layer):
         mask = rising[0]
@@ -340,27 +355,27 @@
     advance(min(4, last))
     normalise(0)
     for layer in range(layers):
-        base = (layer + 1) * last
+        base = offsets[2 * layer] + last
         if layer == 0:
             for own in own_copies:
                 own.wait()
         advance(base + 1)
         gated(layer)
-        advance(base + 2)
+        advance(base + 1 + conv_a)
         halo_arrive(layer)
         convolve(layer, 0)
-        advance(base + min(3, lag))
+        advance(base + 1 + conv_b)
         convolve(layer, 1)
         stat_start(layer)
-        advance(base + lag + 1)
+        advance(offsets[2 * layer + 1] + last + 1)
         activate(layer)
         reduce_start(layer)
         if layer + 1 < layers:
-            advance(base + lag + 2)
+            advance(clock[0] + wait_sum)
             reduce_end(layer, current, middle.at[layer])
             current = middle.at[layer]
             share_start(layer + 1, current)
-            advance(base + lag + 3)
+            advance(clock[0] + wait_share)
             share_relay(layer + 1, current)
             normalise(layer + 1)
         else:
@@ -393,7 +408,9 @@
     layers, rows, width = w_value.shape
     taps = conv_taps.shape[1]
     features = rows * count
-    stages = ring_chunks(layers, rows, width)
+    columns = w_out.shape[2]
+    stages = ring_chunks(layers, rows, width, columns)
+    outward = w_out if columns % LANES == 0 else jnp.swapaxes(w_out, 1, 2)
     pieces = sum(len(stage) for stage in stages)
     dma = pltpu.SemaphoreType.DMA
     return pl.pallas_call(
@@ -402,7 +419,8 @@
         in_specs=[pl.BlockSpec(memory_space=pltpu.VMEM)] * 7,
         out_specs=pl.BlockSpec(memory_space=pltpu.VMEM),
         scratch_shapes=[
-            pltpu.VMEM((3, layers, features, width), BF16),
+            pltpu.VMEM((2, layers, features, width), BF16),
+            pltpu.VMEM((layers, count, *outward.shape[1:]), BF16),
             pltpu.VMEM((layers, peers, tokens, part), BF16),
             pltpu.VMEM((tokens, features), BF16),
             pltpu.VMEM((layers, tokens, width), BF16),
@@ -430,7 +448,7 @@
         compiler_params=pltpu.CompilerParams(
             collective_id=0, has_side_effects=True, vmem_limit_bytes=60 * 1024 * 1024
         ),
-    )(stream, norm_gain, w_value, w_gate, conv_taps, channel_gain, jnp.swapaxes(w_out, 1, 2))
+    )(stream, norm_gain, w_value, w_gate, conv_taps, channel_gain, outward)
 
 
 def solution(mesh):

time: 105 us -> 96.2 us (0.916)
  Pallas kernels: 101 us -> 94.3 us
  local copies, waits for them, and re-layouts: 3.46 us -> 1.67 us
    pallas_call x1, Pallas kernels: 101 us -> 94.3 us  [shards(): pl.pallas_call(functools.partial(kernel, count, peers, stages), out_shape...]
    unnamed x2 -> x1, local copies, waits for them, and re-layouts: 3.46 us -> 1.67 us
where the time goes in v2:
time: 96.2 us; the launch traced here: 96 us
  Pallas kernels  94.3 us (98%)
  local copies, waits for them, and re-layouts  1.67 us (2%)
    pallas_call x1, Pallas kernels, shards(): pl.pallas_call(functools.partial(kernel, count, peers, stages), out_shape...  94.3 us

profile of v2, /device:TPU:0, one launch (start us, length us, event | category | flops | bytes accessed | tf_op | source)
XLA Modules:
  0.0 96.0 jit_solution(465904420009680903)
XLA Ops:
  0.0 94.3 %shard_map.73 = bf16[256,512]{1,0:T(8,128)(2,1)} custom-call(bf16[256,512]{1,0:T(8,128)(2,1)} %x_ref.1, f32[2,2048]{1,0:T(2,128)} %gain_ref.1, bf16[2,256,256]{2,1,0:T(8,128)(2,1)} %wv_ref.1, bf16[2,256,256]{2,1,0:T(8,128)(2,1)} %wg_ref.1, f32[2,128,256]{2,1,0:T(8,128)} %taps_ref.1, f32[2,256]{1,0:T(2,128)} %channel_ref.1, bf16[2,256,256]{2,1,0:T(8,128)(2,1)} %wo_ref.1), custom_call_target="tpu_custom_call" | custom-call | tf_op jit(solution)/shard_map/pallas_call | solution.py:416
  94.3 1.7 %copy.9 = bf16[256,512]{1,0:T(8,128)(2,1)} copy(bf16[256,512]{1,0:T(8,128)(2,1)} %shard_map.73) | data formatting | bytes 524288

commit v3 on v2

--- a/solution.py
+++ b/solution.py
@@ -11,7 +11,7 @@
 LANES = 128
 ROW_TILE = 16
 MESH = pl.DeviceIdType.MESH
-PLAN = (3, 0, 3, 1, 2, 2, 2)
+PLAN = (3, 0, 3, 1, 2, 2, 1)
 
 
 def span(masks):
@@ -348,11 +348,41 @@
                     sum_copy(layer, rising[level + 1], sub ^ rising[level + 1]).start()
         target[...] = (source[...].astype(F32) + mine[0]).astype(BF16)
 
+    joined = len(rising) == 2
+    near, high = rising[0], rising[-1]
+
+    def cross_copy(layer, sub):
+        return pltpu.make_async_remote_copy(
+            src_ref=leaving.at[layer, sub],
+            dst_ref=landing.at[layer, sub ^ high],
+            send_sem=sum_send.at[layer, sub],
+            recv_sem=sum_recv.at[layer, sub ^ high],
+            device_id=(s, partner(high)),
+            device_id_type=MESH,
+        )
+
+    def spread_start(layer):
+        for sub in (high, 0):
+            leaving[layer, near ^ sub] = product(layer, near ^ sub).astype(BF16)
+            sum_copy(layer, near, sub).start()
+        for sub in (high, 0):
+            own_part = product(layer, sub)
+            sum_copy(layer, near, sub).wait_recv()
+            leaving[layer, sub] = (own_part + landing[layer, near ^ sub].astype(F32)).astype(BF16)
+            cross_copy(layer, sub).start()
+
+    def spread_end(layer, sub):
+        cross_copy(layer, sub ^ high).wait_recv()
+        whose = partner(sub)
+        both = leaving[layer, sub].astype(F32) + landing[layer, sub].astype(F32)
+        gathered[layer + 1, whose] = (gathered[layer, whose].astype(F32) + both).astype(BF16)
+        share_copy(layer + 1, gathered.at[layer + 1, whose], near, sub).start()
+
     current = x_ref
     share_start(0, current)
-    advance(min(3, last))
+    advance(min(5, last))
     share_relay(0, current)
-    advance(min(4, last))
+    advance(min(6, last))
     normalise(0)
     for layer in range(layers):
         base = offsets[2 * layer] + last
@@ -369,6 +399,17 @@
         stat_start(layer)
         advance(offsets[2 * layer + 1] + last + 1)
         activate(layer)
+        if joined and layer + 1 < layers:
+            spread_start(layer)
+            advance(clock[0] + wait_sum)
+            spread_end(layer, 0)
+            advance(clock[0] + wait_share)
+            spread_end(layer, high)
+            for sub in (0, high):
+                share_copy(layer + 1, gathered.at[layer + 1, t], near, sub).wait_recv()
+            normalise(layer + 1)
+            current = gathered.at[layer + 1, t]
+            continue
         reduce_start(layer)
         if layer + 1 < layers:
             advance(clock[0] + wait_sum)
@@ -383,12 +424,20 @@
 
     for layer in range(layers):
         source = x_ref if layer == 0 else middle.at[layer - 1]
-        share_end(layer, source)
+        if joined and layer:
+            for sub in (0, high):
+                share_copy(layer, gathered.at[layer, t], near, sub).wait_send()
+        else:
+            share_end(layer, source)
         for bits in range(1, peers):
             stat_copy(layer, bits).wait_send()
         for level, mask in enumerate(rising):
             for sub in span(rising[level + 1 :]):
-                sum_copy(layer, mask, sub).wait_send()
+                if joined and layer + 1 < layers and level:
+                    cross_copy(layer, 0).wait_send()
+                    cross_copy(layer, high).wait_send()
+                else:
+                    sum_copy(layer, mask, sub).wait_send()
 
         @pl.when(s < last)
         def _(layer=layer):

time: 96.2 us -> 94.7 us (0.984)
  Pallas kernels: 94.3 us -> 92.9 us
    pallas_call x1, Pallas kernels: 94.3 us -> 92.9 us  [shards(): pl.pallas_call(functools.partial(kernel, count, peers, stages), out_shape...]
where the time goes in v3:
time: 94.7 us; the launch traced here: 94.6 us
  Pallas kernels  92.9 us (98%)
  local copies, waits for them, and re-layouts  1.67 us (2%)
    pallas_call x1, Pallas kernels, shards(): pl.pallas_call(functools.partial(kernel, count, peers, stages), out_shape...  92.9 us

profile of v3, /device:TPU:0, one launch (start us, length us, event | category | flops | bytes accessed | tf_op | source)
XLA Modules:
  0.0 94.6 jit_solution(2009469294256255087)
XLA Ops:
  0.0 92.9 %shard_map.73 = bf16[256,512]{1,0:T(8,128)(2,1)} custom-call(bf16[256,512]{1,0:T(8,128)(2,1)} %x_ref.1, f32[2,2048]{1,0:T(2,128)} %gain_ref.1, bf16[2,256,256]{2,1,0:T(8,128)(2,1)} %wv_ref.1, bf16[2,256,256]{2,1,0:T(8,128)(2,1)} %wg_ref.1, f32[2,128,256]{2,1,0:T(8,128)} %taps_ref.1, f32[2,256]{1,0:T(2,128)} %channel_ref.1, bf16[2,256,256]{2,1,0:T(8,128)(2,1)} %wo_ref.1), custom_call_target="tpu_custom_call" | custom-call | tf_op jit(solution)/shard_map/pallas_call | solution.py:465
  92.9 1.7 %copy.9 = bf16[256,512]{1,0:T(8,128)(2,1)} copy(bf16[256,512]{1,0:T(8,128)(2,1)} %shard_map.73) | data formatting | bytes 524288
